TPU v7x, 32 devices: a whole 2x2x4 slice. The times are simulated.
32 devices in a mesh: sp: 16 (over z, y, x), tp: 2 (over core).
Axes of the slice: x: 2, y: 2, z: 4, core: 2. Of those that a mesh axis runs over, the one named last changes fastest.
Arguments:
- query_rows: bfloat16 [4096, 1024], P('sp', 'tp'), may hold values from -26 to 26
- key_rows: bfloat16 [4096, 128], P('sp', 'tp'), may hold values from -26 to 26
- value_head_rows: bfloat16 [4096, 128], P('sp', 'tp'), may hold values from -6 to 6
- sink_logit_head: float32 [16], P('tp'), may hold values from -6 to 6
- out_weight: bfloat16 [1024, 2048], P('tp'), may hold values from -0.1875 to 0.1875
- residual: bfloat16 [4096, 2048], P(('sp', 'tp')), may hold values from -6 to 6
- norm_gain: float32 [2048], replicated, may hold values from 0.1 to 1.9
- routes: int32 [4096, 2], P(('sp', 'tp')), may hold values from 0 to 15, all different within a row; in each aligned block of 128 rows (0 to 127, 128 to 255, ...) at most 24 rows name the same one
- route_weights: float32 [4096, 2], P(('sp', 'tp')), may hold values from 0.1 to 1
- gate_proj: bfloat16 [16, 2048, 3584], P('sp', None, 'tp'), may hold values from -0.125 to 0.125
- up_proj: bfloat16 [16, 2048, 3584], P('sp', None, 'tp'), may hold values from -0.125 to 0.125
- down_proj: bfloat16 [16, 3584, 2048], P('sp', 'tp'), may hold values from -0.09375 to 0.09375
Outputs:
- output: bfloat16 [4096, 2048], P(('sp', 'tp'))
Inputs may be any that keep to these rules, and one draw needn't show every extreme that they name: `routes`: A row names 2 different experts. Among the rows of one device no expert is named more than 24 times, a bound that some block reaches on some devices.
All inputs are finite; a program needn't handle non-finite values.
Results may differ from a plain program's by a relative error of at most 0.0055.
Values may be sent and summed in bfloat16 or wider, within the bound.
No kernel may reach another device: no remote copies, remote signals or barrier semaphores. Data moves between devices by JAX's collectives and lax.ppermute only.
A program may use at most 128 MiB of HBM per device.

v0:
```python
import jax
import jax.numpy as jnp
from jax import lax
from jax.sharding import PartitionSpec as P

QUERY_HEADS = 16
KEY_VALUE_HEADS = 2
HEAD_SIZE = 64
TOP = 2
WINDOW_KEYS = 128


def from_behind(block, axis, distance):
    devices = range(lax.axis_size(axis))
    route = [(i - distance, i) for i in devices if i - distance in devices]
    return lax.ppermute(block, axis, route)


def on_device(
    query_rows,
    key_rows,
    value_head_rows,
    sink_logit_head,
    out_weight,
    residual,
    norm_gain,
    routes,
    route_weights,
    gate_proj,
    up_proj,
    down_proj,
):
    length = query_rows.shape[0]
    query_group = QUERY_HEADS // KEY_VALUE_HEADS
    width = key_rows.shape[1]
    local_kv = width // HEAD_SIZE
    local_heads = local_kv * query_group
    sp_index = lax.axis_index("sp")
    tp_index = lax.axis_index("tp")
    tail = jnp.concatenate(
        [key_rows[length - WINDOW_KEYS :], value_head_rows[length - WINDOW_KEYS :]], axis=1
    )
    before = from_behind(tail, "sp", 1)
    key_all = jnp.concatenate([before[:, :width], key_rows], axis=0)
    value_all = jnp.concatenate([before[:, width:], value_head_rows], axis=0)
    score_matrix = jnp.einsum(
        "rjwh,cjh->jwrc",
        query_rows.reshape(length, local_kv, query_group, HEAD_SIZE),
        key_all.reshape(-1, local_kv, HEAD_SIZE),
        preferred_element_type=jnp.float32,
    ) * HEAD_SIZE ** (-0.5)
    query_pos = sp_index * length + jnp.arange(length, dtype=jnp.int32)
    key_pos = sp_index * length - WINDOW_KEYS + jnp.arange(length + WINDOW_KEYS, dtype=jnp.int32)
    distance = query_pos[:, None] - key_pos[None, :]
    inside = (distance >= 0) & (distance < WINDOW_KEYS) & (key_pos[None, :] >= 0)
    head_ids = (tp_index * local_heads + jnp.arange(local_heads, dtype=jnp.int32)).astype(
        jnp.float32
    )
    slope_values = jnp.exp2(-8.0 * (head_ids + 1.0) / QUERY_HEADS).reshape(local_kv, query_group)
    score_matrix = (
        score_matrix - slope_values[:, :, None, None] * distance.astype(jnp.float32)[None, None]
    )
    score_matrix = jnp.where(inside[None, None], score_matrix, -jnp.inf)
    sink_portion = sink_logit_head.reshape(local_kv, query_group)[:, :, None]
    peak = jnp.maximum(jnp.max(score_matrix, axis=-1), sink_portion)
    expd = jnp.exp(score_matrix - peak[..., None])
    denom = jnp.sum(expd, axis=-1) + jnp.exp(sink_portion - peak)
    probabilities = (expd / denom[..., None]).astype(jnp.bfloat16)
    attended = (
        jnp.einsum(
            "wfbt,twj->bwfj",
            probabilities,
            value_all.reshape(-1, local_kv, HEAD_SIZE),
            preferred_element_type=jnp.float32,
        )
        .reshape(length, local_heads * HEAD_SIZE)
        .astype(jnp.bfloat16)
    )
    own_rows = length // lax.axis_size("tp")
    projected = lax.psum_scatter(
        jnp.dot(attended, out_weight, preferred_element_type=jnp.float32),
        "tp",
        scatter_dimension=0,
        tiled=True,
    )
    mixed = residual.astype(jnp.float32) + projected
    scale = lax.rsqrt(jnp.mean(mixed * mixed, axis=-1, keepdims=True) + 1e-05)
    normed = (mixed * scale * norm_gain).astype(jnp.bfloat16)
    n_sp = lax.axis_size("sp")
    n_tp = lax.axis_size("tp")
    capacity = 3 * own_rows * TOP // (2 * n_sp)
    chosen = routes.reshape(-1)
    onehot = (chosen[:, None] == jnp.arange(n_sp, dtype=jnp.int32)[None, :]).astype(jnp.int32)
    running = jnp.cumsum(onehot, axis=0)
    rank_in = jnp.sum(onehot * running, axis=1) - 1
    slot_index = chosen * capacity + rank_in
    slot_ids = jnp.arange(n_sp * capacity, dtype=jnp.int32)
    select = jnp.any(
        slot_index.reshape(own_rows, TOP)[None, :, :] == slot_ids[:, None, None], axis=-1
    )
    dispatch = jnp.dot(
        select.astype(jnp.bfloat16), normed, preferred_element_type=jnp.float32
    ).astype(jnp.bfloat16)
    model_width = dispatch.shape[1]
    landed = lax.all_to_all(
        dispatch.reshape(n_sp, capacity, model_width), "sp", split_axis=0, concat_axis=0, tiled=True
    )
    arrived = lax.all_gather(
        landed.reshape(n_sp, 1, capacity, model_width), "tp", axis=1, tiled=True
    )
    rows_in = arrived.reshape(-1, model_width)
    gate = jnp.dot(rows_in, gate_proj[0], preferred_element_type=jnp.float32)
    upper = jnp.dot(rows_in, up_proj[0], preferred_element_type=jnp.float32)
    hidden = (jax.nn.silu(gate) * upper).astype(jnp.bfloat16)
    partial_out = jnp.dot(hidden, down_proj[0], preferred_element_type=jnp.float32)
    partial_out = partial_out.reshape(n_sp, n_tp, capacity, model_width)
    summed = lax.psum_scatter(
        partial_out.astype(jnp.bfloat16), "tp", scatter_dimension=1, tiled=True
    )
    expert_out = summed.reshape(n_sp, capacity, model_width)
    returned = lax.all_to_all(expert_out, "sp", split_axis=0, concat_axis=0, tiled=True)
    picked = returned.reshape(n_sp * capacity, model_width)[slot_index].reshape(
        own_rows, TOP, model_width
    )
    moe_sum = jnp.sum(route_weights[:, :, None] * picked.astype(jnp.float32), axis=1)
    return (mixed + moe_sum).astype(jnp.bfloat16)


def solution(mesh):
    placed = (
        P("sp", "tp"),
        P("sp", "tp"),
        P("sp", "tp"),
        P("tp"),
        P("tp", None),
        P(("sp", "tp"), None),
        P(),
        P(("sp", "tp"), None),
        P(("sp", "tp"), None),
        P("sp", None, "tp"),
        P("sp", None, "tp"),
        P("sp", "tp", None),
    )
    return jax.shard_map(
        on_device, mesh=mesh, in_specs=placed, out_specs=P(("sp", "tp"), None), check_vma=False
    )
```

profile of v0, /device:TPU:12, one launch (start us, length us, event | category | flops | bytes accessed | tf_op | source)
XLA Modules:
  0.0 209.4 jit_solution(3881032120100905958)
XLA Ops:
  6.5 0.9 slice.18
  7.4 0.7 slice.19
  8.1 3.4 %collective-permute-start = (bf16[128,128]{0,1:T(8,128)(2,1)S(1)}, bf16[128,128]{0,1:T(8,128)(2,1)S(1)}, u32[]{:S(2)}, u32[]{:S(2)}) collective-permute-start(bf16[128,128]{0,1:T(8,128)(2,1)S(1)} %pad_maximum_fusion), channel_id=1, source_target_pairs={{0,2},{2,4},{4,6},{6,8},{8,10},{10,12},{12,14},{14,16},{16,18},{18... | collective-permute-start | bytes 98312 | tf_op jit(solution)/shard_map/ppermute | solution.py:16
  11.7 0.2 fusion.22
  11.9 1.1 copy.31
  13.0 1.8 collective-permute-done
  14.8 1.6 fusion.34
  16.5 0.4 fusion.12
  17.0 0.7 fusion.15
  17.8 2.1 fusion.35
  20.3 0.6 reduce-window.6
  20.9 0.2 slice_reduce_fusion
  21.2 0.1 sub.63
  21.5 8.8 %reduce-scatter.3.cloned.1.call-done = f32[128,2048]{1,0:T(8,128)} async-done(((f32[256,2048]{1,0:T(8,128)}), f32[128,2048]{1,0:T(8,128)}) %reduce-scatter.3.cloned.1.call-update) | async-done | bytes 1048592 | tf_op jit(solution)/shard_map/reduce_scatter | solution.py:80
  30.4 1.4 multiply_reduce_fusion.1
  31.8 1.9 convolution_convert_fusion
  33.7 43.6 %all_to_all.10 = bf16[16,24,2048]{2,1,0:T(8,128)(2,1)} all-to-all(bf16[16,24,2048]{2,1,0:T(8,128)(2,1)S(1)} %bitcast.75), channel_id=1, replica_groups=mesh['sp'=16,'tp'=2] {'sp'}, dimensions={0} | all-to-all | bytes 3145728 | tf_op jit(solution)/shard_map/all_to_all | solution.py:105
  77.3 0.2 all-reduce.3.cloned.1.call-start
  77.5 11.4 %all-gather.3.cloned.1.call-done = bf16[16,48,2048]{2,1,0:T(8,128)(2,1)} async-done(((bf16[16,24,2048]{2,1,0:T(8,128)(2,1)}), bf16[16,48,2048]{2,1,0:T(8,128)(2,1)}) %all-gather.3.cloned.1.call-update) | async-done | bytes 3145744 | tf_op jit(solution)/shard_map/all_gather | solution.py:108
  88.9 10.0 %fusion.4 = f32[768,1792]{1,0:T(8,128)S(1)} fusion(bf16[768,2048]{1,0:T(8,128)(2,1)} %bitcast.82, bf16[1,2048,1792]{2,1,0:T(8,128)(2,1)} %param.21), kind=kOutput, calls=%fused_computation.5 | convolution fusion | flops 5637144576 | bytes 15990784 | tf_op jit(solution)/shard_map/dot_general | solution.py:112
  98.9 9.7 %multiply_convert_fusion = bf16[768,1792]{1,0:T(8,128)(2,1)S(1)} fusion(f32[768,1792]{1,0:T(8,128)S(1)} %fusion.4, bf16[768,2048]{1,0:T(8,128)(2,1)S(1)} %bitcast.83, bf16[1,2048,1792]{2,1,0:T(8,128)(2,1)} %param.22), kind=kOutput, calls=%fused_computation.7 | convolution fusion | flops 5645402112 | bytes 18743296 | tf_op jit(solution)/shard_map/dot_general | solution.py:113
  108.7 7.3 %fusion.8 = bf16[16,2,24,2048]{3,2,1,0:T(8,128)(2,1)} fusion(bf16[16,2,24,1792]{3,2,1,0:T(8,128)(2,1)S(1)} %bitcast.84, bf16[1,1792,2048]{2,1,0:T(8,128)(2,1)S(1)} %bitcast.81), kind=kOutput, calls=%fused_computation.8 | convolution fusion | flops 5638717440 | bytes 13238272 | tf_op jit(solution)/shard_map/dot_general | solution.py:115
  116.1 0.6 copy-done.10
  116.7 0.6 dynamic-slice
  117.3 23.4 %all-reduce.3.cloned.1.call-done = bf16[16,2,24,2048]{3,2,1,0:T(8,128)(2,1)} async-done(((bf16[16,2,24,2048]{3,2,1,0:T(8,128)(2,1)}), bf16[16,2,24,2048]{3,2,1,0:T(8,128)(2,1)}) %all-reduce.3.cloned.1.call-update) | async-done | bytes 3145744
  140.7 3.4 %dynamic-slice_bitcast_fusion = bf16[16,24,2048]{2,1,0:T(8,128)(2,1)} fusion(bf16[16,2,24,2048]{3,2,1,0:T(8,128)(2,1)} %all-reduce.3.cloned.1.call-done, u32[]{:T(128)} %bitcast.29), kind=kLoop, calls=%fused_computation.16 | loop fusion | bytes 3145732 | tf_op jit(solution)/shard_map/reshape | solution.py:120
  144.1 7.0 %all-to-all-start.1 = ((bf16[16,24,2048]{2,1,0:T(8,128)(2,1)}), bf16[16,24,2048]{2,1,0:T(8,128)(2,1)}, u32[]{:S(2)}, u32[]{:S(2)}) async-start(bf16[16,24,2048]{2,1,0:T(8,128)(2,1)} %dynamic-slice_bitcast_fusion), calls=%async_computation.2 | async-start | bytes 3145728 | tf_op jit(solution)/shard_map/all_to_all | solution.py:121
  151.3 37.2 %all-to-all-done.1 = bf16[16,24,2048]{2,1,0:T(8,128)(2,1)} async-done(((bf16[16,24,2048]{2,1,0:T(8,128)(2,1)}), bf16[16,24,2048]{2,1,0:T(8,128)(2,1)}, u32[]{:S(2)}, u32[]{:S(2)}) %all-to-all-start.1) | async-done | bytes 1572896 | tf_op jit(solution)/shard_map/all_to_all | solution.py:121
  188.5 5.0 %gather_fusion = bf16[256,2048]{1,0:T(8,128)(2,1)} fusion(bf16[384,2048]{1,0:T(8,128)(2,1)} %bitcast.19, s32[1024]{0:T(1024)S(1)} %pad_clamp_fusion), kind=kCustom, calls=%fused_computation | custom fusion | bytes 2098176 | tf_op jit(solution)/shard_map/gather | solution.py:122
  193.5 3.5 %reshape.286 = f32[128,2,2048]{2,1,0:T(2,128)} reshape(bf16[256,2048]{1,0:T(8,128)(2,1)} %gather_fusion) | data formatting | bytes 3145728 | tf_op jit(solution)/shard_map/convert_element_type | solution.py:125
  197.0 4.9 %multiply_reduce_fusion = f32[128,2048]{1,0:T(8,128)S(1)} fusion(f32[128,2,2048]{2,1,0:T(2,128)} %reshape.286, f32[128,2]{1,0:T(8,128)S(1)} %copy.33), kind=kLoop, calls=%fused_computation.15 | loop fusion | flops 786432 | bytes 3146752 | tf_op jit(solution)/shard_map/reduce_sum | solution.py:125
  201.9 1.0 add_convert_fusion
  (56 shorter events, 1.4 us)
Async XLA Ops:
  6.5 11.2 %copy-start = (bf16[512,2048]{1,0:T(8,128)(2,1)S(1)}, bf16[512,2048]{1,0:T(8,128)(2,1)}, u32[]{:S(2)}) copy-start(bf16[512,2048]{1,0:T(8,128)(2,1)} %param.16) | copy-start | bytes 6291460
  6.5 9.9 %copy-start.6 = (f32[8]{0:T(128)S(1)}, f32[8]{0:T(128)}, u32[]{:S(2)}) copy-start(f32[8]{0:T(128)} %param.15) | copy-start | bytes 100
  6.5 23.8 %reduce-scatter.3.cloned.1.call-start = ((), (), s32[]{:S(2)}) async-start(), calls=%async_computation.3 | async-start | bytes 3145728 | tf_op jit(solution)/shard_map/reduce_scatter | solution.py:80
  8.1 6.7 %collective-permute-start = (bf16[128,128]{0,1:T(8,128)(2,1)S(1)}, bf16[128,128]{0,1:T(8,128)(2,1)S(1)}, u32[]{:S(2)}, u32[]{:S(2)}) collective-permute-start(bf16[128,128]{0,1:T(8,128)(2,1)S(1)} %pad_maximum_fusion), channel_id=1, source_target_pairs={{0,2},{2,4},{4,6},{6,8},{8,10},{10,12},{12,14},{14,16},{16,18},{18... | collective-permute-start | bytes 98312 | tf_op jit(solution)/shard_map/ppermute | solution.py:16
  14.8 2.2 %copy-start.5 = (bf16[256,64]{0,1:T(8,128)(2,1)S(1)}, bf16[256,64]{0,1:T(8,128)(2,1)}, u32[]{:S(2)}) copy-start(bf16[256,64]{0,1:T(8,128)(2,1)} %param.14) | copy-start | bytes 98308
  17.7 2.2 %copy-start.7 = (s32[128,2]{0,1:T(2,128)S(1)}, s32[128,2]{0,1:T(2,128)}, u32[]{:S(2)}) copy-start(s32[128,2]{0,1:T(2,128)} %param.19) | copy-start | bytes 3076
  17.7 12.6 %copy-start.2 = (bf16[128,2048]{1,0:T(8,128)(2,1)S(1)}, bf16[128,2048]{1,0:T(8,128)(2,1)}, u32[]{:S(2)}) copy-start(bf16[128,2048]{1,0:T(8,128)(2,1)} %param.17) | copy-start | bytes 1572868
  19.8 12.0 %copy-start.4 = (f32[2048]{0:T(1024)S(1)}, f32[2048]{0:T(1024)}, u32[]{:S(2)}) copy-start(f32[2048]{0:T(1024)} %param.18) | copy-start | bytes 24580
  19.9 69.0 %all-gather.3.cloned.1.call-start = ((), (), s32[]{:S(2)}) async-start(), calls=%async_computation.4 | async-start | bytes 4718592 | tf_op jit(solution)/shard_map/all_gather | solution.py:108
  77.3 63.4 %all-reduce.3.cloned.1.call-start = ((), (), s32[]{:S(2)}) async-start(), calls=%async_computation.5 | async-start | bytes 6291456
  88.9 10.0 %copy-start.9 = (bf16[16,48,2048]{2,1,0:T(8,128)(2,1)S(1)}, bf16[16,48,2048]{2,1,0:T(8,128)(2,1)}, u32[]{:S(2)}) copy-start(bf16[16,48,2048]{2,1,0:T(8,128)(2,1)} %all-gather.3.cloned.1.call-done) | copy-start | bytes 9437188
  88.9 19.8 %slice-start = ((s8[7340032]{0:T(1024)(128)(4,1)}), s8[4194304]{0:T(1024)(128)(4,1)S(1)}, s32[]{:S(2)}) async-start(s8[7340032]{0:T(1024)(128)(4,1)} %bitcast.80), calls=%async_computation.6 | async-start | bytes 8388608
  98.9 9.7 %slice-start.1 = ((s8[7340032]{0:T(1024)(128)(4,1)}), s8[3145728]{0:T(1024)(128)(4,1)S(1)}, s32[]{:S(2)}) async-start(s8[7340032]{0:T(1024)(128)(4,1)} %bitcast.80), calls=%async_computation.7 | async-start | bytes 6291456
  116.0 0.7 copy-start.10
  140.7 10.5 %copy-start.8 = (f32[128,2]{0,1:T(2,128)S(1)}, f32[128,2]{0,1:T(2,128)}, u32[]{:S(2)}) copy-start(f32[128,2]{0,1:T(2,128)} %param.20) | copy-start | bytes 3076
  144.1 44.5 %all-to-all-start.1 = ((bf16[16,24,2048]{2,1,0:T(8,128)(2,1)}), bf16[16,24,2048]{2,1,0:T(8,128)(2,1)}, u32[]{:S(2)}, u32[]{:S(2)}) async-start(bf16[16,24,2048]{2,1,0:T(8,128)(2,1)} %dynamic-slice_bitcast_fusion), calls=%async_computation.2 | async-start | bytes 3145728 | tf_op jit(solution)/shard_map/all_to_all | solution.py:121
  193.5 8.4 %copy-start.1 = (f32[128,2048]{1,0:T(8,128)S(1)}, f32[128,2048]{1,0:T(8,128)}, u32[]{:S(2)}) copy-start(f32[128,2048]{1,0:T(8,128)} %reduce-scatter.3.cloned.1.call-done) | copy-start | bytes 3145732
  197.0 4.9 %copy-start.3 = (bf16[128,2048]{1,0:T(8,128)(2,1)S(1)}, bf16[128,2048]{1,0:T(8,128)(2,1)}, u32[]{:S(2)}) copy-start(bf16[128,2048]{1,0:T(8,128)(2,1)} %param.17) | copy-start | bytes 1572868
Sparse Core Ops, SparseCore 0:
  20.0 10.3 reduce-scatter.2
  77.4 11.4 all-gather.2
  116.2 24.4 all-reduce.2
where the time goes:
time: 210 us; the launch traced here: 209 us
  waiting for transfers between devices  82.7 us (39%)
  blocking collectives  43.6 us (21%)
  matrix products  33.3 us (16%)
  local copies, waits for them, and re-layouts  16.8 us (8%)
  between operations  13.4 us (6%)
  starting transfers between devices  10.6 us (5%)
  other arithmetic  9.03 us (4%)
    all_to_all x1, blocking collectives, on_device(): lax.all_to_all(dispatch.reshape(n_sp, capacity, model_width), 'sp', split...  43.6 us
    all_to_all x1, waiting for transfers between devices, on_device(): lax.all_to_all(expert_out, 'sp', split_axis=0, concat_axis=0, tiled=True)  37.2 us
    unnamed x4, waiting for transfers between devices  23.5 us
    all_gather x1, waiting for transfers between devices, on_device(): lax.all_gather(landed.reshape(n_sp, 1, capacity, model_width), 'tp', axis...  11.4 us
    dot_general x1, matrix products, on_device(): gate = jnp.dot(rows_in, gate_proj[0], preferred_element_type=jnp.float32)  10 us
    dot_general x1, matrix products, on_device(): upper = jnp.dot(rows_in, up_proj[0], preferred_element_type=jnp.float32)  9.71 us
    reduce_scatter x1, waiting for transfers between devices, on_device(): lax.psum_scatter(jnp.dot(attended, out_weight, preferred_element_type=jnp...  8.81 us
    dot_general x1, matrix products, on_device(): jnp.dot(hidden, down_proj[0], preferred_element_type=jnp.float32)  7.35 us
  transfers between devices with their start and end apart: 5, of which 5 were waited for; matrix products, arithmetic and copies ran while one was open for 2% of the time, Pallas kernels for 0%

commit v1 on v0

--- a/solution.py
+++ b/solution.py
@@ -8,6 +8,12 @@
 HEAD_SIZE = 64
 TOP = 2
 WINDOW_KEYS = 128
+
+
+def gathered_along(x, name, dim):
+    parts = lax.all_gather(x, name, axis=0, tiled=False)
+    whole = jnp.concatenate(parts, axis=dim)
+    return whole
 
 
 def from_behind(block, axis, distance):
@@ -105,9 +111,7 @@
     landed = lax.all_to_all(
         dispatch.reshape(n_sp, capacity, model_width), "sp", split_axis=0, concat_axis=0, tiled=True
     )
-    arrived = lax.all_gather(
-        landed.reshape(n_sp, 1, capacity, model_width), "tp", axis=1, tiled=True
-    )
+    arrived = gathered_along(landed.reshape(n_sp, 1, capacity, model_width), "tp", 1)
     rows_in = arrived.reshape(-1, model_width)
     gate = jnp.dot(rows_in, gate_proj[0], preferred_element_type=jnp.float32)
     upper = jnp.dot(rows_in, up_proj[0], preferred_element_type=jnp.float32)

time: 210 us -> 208 us (level)
  matrix products: 33.3 us -> 29.1 us
  local copies, waits for them, and re-layouts: 16.8 us -> 19.1 us
    dot_general x1, matrix products: 9.71 us -> 6.43 us  [on_device(): upper = jnp.dot(rows_in, up_proj[0], preferred_element_type=jnp.float32)]
    reshape x0 -> x1, local copies, waits for them, and re-layouts: none -> 2.26 us  [gathered_along(): whole = jnp.concatenate(parts, axis=dim)]
where the time goes in v1:
time: 208 us
  waiting for transfers between devices  82.7 us (40%)
  blocking collectives  43.6 us (21%)
  matrix products  29.1 us (14%)
  local copies, waits for them, and re-layouts  19.1 us (9%)
  between operations  13.4 us (6%)
  starting transfers between devices  10.6 us (5%)
  other arithmetic  9.03 us (4%)
    all_to_all x1, blocking collectives, on_device(): lax.all_to_all(dispatch.reshape(n_sp, capacity, model_width), 'sp', split...  43.6 us
    all_to_all x1, waiting for transfers between devices, on_device(): lax.all_to_all(expert_out, 'sp', split_axis=0, concat_axis=0, tiled=True)  37.2 us
    unnamed x4, waiting for transfers between devices  23.5 us
    all_gather x1, waiting for transfers between devices, gathered_along(): parts = lax.all_gather(x, name, axis=0, tiled=False)  11.4 us
    dot_general x1, matrix products, on_device(): gate = jnp.dot(rows_in, gate_proj[0], preferred_element_type=jnp.float32)  9.08 us
    reduce_scatter x1, waiting for transfers between devices, on_device(): lax.psum_scatter(jnp.dot(attended, out_weight, preferred_element_type=jnp...  8.81 us
    dot_general x1, matrix products, on_device(): jnp.dot(hidden, down_proj[0], preferred_element_type=jnp.float32)  7.39 us
    all_to_all x1, starting transfers between devices, on_device(): lax.all_to_all(expert_out, 'sp', split_axis=0, concat_axis=0, tiled=True)  6.96 us
  transfers between devices with their start and end apart: 5, of which 5 were waited for; matrix products, arithmetic and copies ran while one was open for 2% of the time, Pallas kernels for 0%

profile of v1, /device:TPU:12, one launch (start us, length us, event | category | flops | bytes accessed | tf_op | source)
XLA Modules:
  0.0 207.5 jit_solution(2342490488179488316)
XLA Ops:
  6.5 0.9 slice.18
  7.4 0.7 slice.19
  8.1 3.4 %collective-permute-start = (bf16[128,128]{0,1:T(8,128)(2,1)S(1)}, bf16[128,128]{0,1:T(8,128)(2,1)S(1)}, u32[]{:S(2)}, u32[]{:S(2)}) collective-permute-start(bf16[128,128]{0,1:T(8,128)(2,1)S(1)} %pad_maximum_fusion), channel_id=1, source_target_pairs={{0,2},{2,4},{4,6},{6,8},{8,10},{10,12},{12,14},{14,16},{16,18},{18... | collective-permute-start | bytes 98312 | tf_op jit(solution)/shard_map/ppermute | solution.py:22
  11.7 0.2 fusion.22
  11.9 1.1 copy.40
  13.0 1.8 collective-permute-done
  14.8 1.6 fusion.34
  16.5 0.4 fusion.12
  17.0 0.7 fusion.15
  17.8 2.1 %fusion.35 = f32[256,2048]{1,0:T(8,128)} fusion(bf16[256,512]{0,1:T(8,128)(2,1)S(1)} %bitcast.82, bf16[512,2048]{1,0:T(8,128)(2,1)S(1)} %copy-done), kind=kOutput, calls=%fused_computation.64 | convolution fusion | flops 536870912 | bytes 4456448 | tf_op jit(solution)/shard_map/dot_general | solution.py:87
  20.3 0.6 reduce-window.6
  20.9 0.2 slice_reduce_fusion
  21.5 8.8 %reduce-scatter.3.cloned.1.call-done = f32[128,2048]{1,0:T(8,128)} async-done(((f32[256,2048]{1,0:T(8,128)}), f32[128,2048]{1,0:T(8,128)}) %reduce-scatter.3.cloned.1.call-update) | async-done | bytes 1048592 | tf_op jit(solution)/shard_map/reduce_scatter | solution.py:86
  30.4 1.4 multiply_reduce_fusion.1
  31.8 1.9 convolution_convert_fusion
  33.7 43.6 %all_to_all.10 = bf16[16,24,2048]{2,1,0:T(8,128)(2,1)} all-to-all(bf16[16,24,2048]{2,1,0:T(8,128)(2,1)S(1)} %bitcast.78), channel_id=1, replica_groups=mesh['sp'=16,'tp'=2] {'sp'}, dimensions={0} | all-to-all | bytes 3145728 | tf_op jit(solution)/shard_map/all_to_all | solution.py:111
  77.3 0.2 all-reduce.3.cloned.1.call-start
  77.5 11.4 %all-gather.3.cloned.1.call-done = bf16[32,24,2048]{2,1,0:T(8,128)(2,1)} async-done(((bf16[16,24,2048]{2,1,0:T(8,128)(2,1)}), bf16[32,24,2048]{2,1,0:T(8,128)(2,1)}) %all-gather.3.cloned.1.call-update) | async-done | bytes 3145744 | tf_op jit(solution)/shard_map/all_gather | solution.py:14
  88.9 2.3 %copy.48 = bf16[16,2,1,24,2048]{4,3,1,0,2:T(8,128)(2,1)S(1)} copy(bf16[16,2,1,24,2048]{4,3,0,1,2:T(8,128)(2,1)} %bitcast.79) | data formatting | bytes 6291456 | tf_op jit(solution)/shard_map/reshape | solution.py:15
  91.2 9.1 %fusion.4 = f32[768,1792]{1,0:T(8,128)S(1)} fusion(bf16[768,2048]{1,0:T(8,128)(2,1)S(1)} %bitcast.80, bf16[1,2048,1792]{2,1,0:T(8,128)(2,1)} %param.21), kind=kOutput, calls=%fused_computation.5 | convolution fusion | flops 5637144576 | bytes 15990784 | tf_op jit(solution)/shard_map/dot_general | solution.py:116
  100.3 6.4 %multiply_convert_fusion = bf16[768,1792]{1,0:T(8,128)(2,1)S(1)} fusion(f32[768,1792]{1,0:T(8,128)S(1)} %fusion.4, bf16[768,2048]{1,0:T(8,128)(2,1)S(1)} %bitcast.81, bf16[1,2048,1792]{2,1,0:T(8,128)(2,1)S(1)} %bitcast.87), kind=kOutput, calls=%fused_computation.7 | convolution fusion | flops 5645402112 | bytes 18743296 | tf_op jit(solution)/shard_map/dot_general | solution.py:117
  106.8 7.4 %fusion.8 = bf16[16,2,24,2048]{3,2,1,0:T(8,128)(2,1)} fusion(bf16[16,2,24,1792]{3,2,1,0:T(8,128)(2,1)S(1)} %bitcast.90, bf16[1,1792,2048]{2,1,0:T(8,128)(2,1)S(1)} %bitcast.89), kind=kOutput, calls=%fused_computation.8 | convolution fusion | flops 5638717440 | bytes 13238272 | tf_op jit(solution)/shard_map/dot_general | solution.py:119
  114.2 0.6 copy-done.9
  114.8 0.6 dynamic-slice
  115.4 23.4 %all-reduce.3.cloned.1.call-done = bf16[16,2,24,2048]{3,2,1,0:T(8,128)(2,1)} async-done(((bf16[16,2,24,2048]{3,2,1,0:T(8,128)(2,1)}), bf16[16,2,24,2048]{3,2,1,0:T(8,128)(2,1)}) %all-reduce.3.cloned.1.call-update) | async-done | bytes 3145744
  138.8 3.4 %dynamic-slice_bitcast_fusion = bf16[16,24,2048]{2,1,0:T(8,128)(2,1)} fusion(bf16[16,2,24,2048]{3,2,1,0:T(8,128)(2,1)} %all-reduce.3.cloned.1.call-done, u32[]{:T(128)} %bitcast.32), kind=kLoop, calls=%fused_computation.16 | loop fusion | bytes 3145732 | tf_op jit(solution)/shard_map/reshape | solution.py:124
  142.2 7.0 %all-to-all-start.1 = ((bf16[16,24,2048]{2,1,0:T(8,128)(2,1)}), bf16[16,24,2048]{2,1,0:T(8,128)(2,1)}, u32[]{:S(2)}, u32[]{:S(2)}) async-start(bf16[16,24,2048]{2,1,0:T(8,128)(2,1)} %dynamic-slice_bitcast_fusion), calls=%async_computation.2 | async-start | bytes 3145728 | tf_op jit(solution)/shard_map/all_to_all | solution.py:125
  149.5 37.2 %all-to-all-done.1 = bf16[16,24,2048]{2,1,0:T(8,128)(2,1)} async-done(((bf16[16,24,2048]{2,1,0:T(8,128)(2,1)}), bf16[16,24,2048]{2,1,0:T(8,128)(2,1)}, u32[]{:S(2)}, u32[]{:S(2)}) %all-to-all-start.1) | async-done | bytes 1572896 | tf_op jit(solution)/shard_map/all_to_all | solution.py:125
  186.7 5.0 %gather_fusion = bf16[256,2048]{1,0:T(8,128)(2,1)} fusion(bf16[384,2048]{1,0:T(8,128)(2,1)} %bitcast.21, s32[1024]{0:T(1024)S(1)} %pad_clamp_fusion), kind=kCustom, calls=%fused_computation | custom fusion | bytes 2098176 | tf_op jit(solution)/shard_map/gather | solution.py:126
  191.7 3.5 %reshape.282 = f32[128,2,2048]{2,1,0:T(2,128)} reshape(bf16[256,2048]{1,0:T(8,128)(2,1)} %gather_fusion) | data formatting | bytes 3145728 | tf_op jit(solution)/shard_map/convert_element_type | solution.py:129
  195.1 4.9 %multiply_reduce_fusion = f32[128,2048]{1,0:T(8,128)S(1)} fusion(f32[128,2,2048]{2,1,0:T(2,128)} %reshape.282, f32[128,2]{1,0:T(8,128)S(1)} %copy.42), kind=kLoop, calls=%fused_computation.15 | loop fusion | flops 786432 | bytes 3146752 | tf_op jit(solution)/shard_map/reduce_sum | solution.py:129
  200.0 1.0 add_convert_fusion
  (60 shorter events, 1.5 us)
Async XLA Ops:
  6.5 11.2 %copy-start = (bf16[512,2048]{1,0:T(8,128)(2,1)S(1)}, bf16[512,2048]{1,0:T(8,128)(2,1)}, u32[]{:S(2)}) copy-start(bf16[512,2048]{1,0:T(8,128)(2,1)} %param.16) | copy-start | bytes 6291460
  6.5 9.9 %copy-start.6 = (f32[8]{0:T(128)S(1)}, f32[8]{0:T(128)}, u32[]{:S(2)}) copy-start(f32[8]{0:T(128)} %param.15) | copy-start | bytes 100
  6.5 23.8 %reduce-scatter.3.cloned.1.call-start = ((), (), s32[]{:S(2)}) async-start(), calls=%async_computation.3 | async-start | bytes 3145728 | tf_op jit(solution)/shard_map/reduce_scatter | solution.py:86
  8.1 6.7 %collective-permute-start = (bf16[128,128]{0,1:T(8,128)(2,1)S(1)}, bf16[128,128]{0,1:T(8,128)(2,1)S(1)}, u32[]{:S(2)}, u32[]{:S(2)}) collective-permute-start(bf16[128,128]{0,1:T(8,128)(2,1)S(1)} %pad_maximum_fusion), channel_id=1, source_target_pairs={{0,2},{2,4},{4,6},{6,8},{8,10},{10,12},{12,14},{14,16},{16,18},{18... | collective-permute-start | bytes 98312 | tf_op jit(solution)/shard_map/ppermute | solution.py:22
  14.8 2.2 %copy-start.5 = (bf16[256,64]{0,1:T(8,128)(2,1)S(1)}, bf16[256,64]{0,1:T(8,128)(2,1)}, u32[]{:S(2)}) copy-start(bf16[256,64]{0,1:T(8,128)(2,1)} %param.14) | copy-start | bytes 98308
  17.7 2.2 %copy-start.7 = (s32[128,2]{0,1:T(2,128)S(1)}, s32[128,2]{0,1:T(2,128)}, u32[]{:S(2)}) copy-start(s32[128,2]{0,1:T(2,128)} %param.19) | copy-start | bytes 3076
  17.7 12.6 %copy-start.2 = (bf16[128,2048]{1,0:T(8,128)(2,1)S(1)}, bf16[128,2048]{1,0:T(8,128)(2,1)}, u32[]{:S(2)}) copy-start(bf16[128,2048]{1,0:T(8,128)(2,1)} %param.17) | copy-start | bytes 1572868
  19.8 12.0 %copy-start.4 = (f32[2048]{0:T(1024)S(1)}, f32[2048]{0:T(1024)}, u32[]{:S(2)}) copy-start(f32[2048]{0:T(1024)} %param.18) | copy-start | bytes 24580
  19.9 69.0 %all-gather.3.cloned.1.call-start = ((), (), s32[]{:S(2)}) async-start(), calls=%async_computation.4 | async-start | bytes 4718592 | tf_op jit(solution)/shard_map/all_gather | solution.py:14
  77.3 61.5 %all-reduce.3.cloned.1.call-start = ((), (), s32[]{:S(2)}) async-start(), calls=%async_computation.5 | async-start | bytes 6291456
  88.9 11.4 %slice-start = ((s8[7340032]{0:T(1024)(128)(4,1)}), s8[4194304]{0:T(1024)(128)(4,1)S(1)}, s32[]{:S(2)}) async-start(s8[7340032]{0:T(1024)(128)(4,1)} %bitcast.86), calls=%async_computation.6 | async-start | bytes 8388608
  91.2 9.1 %slice-start.1 = ((s8[7340032]{0:T(1024)(128)(4,1)}), s8[3145728]{0:T(1024)(128)(4,1)S(1)}, s32[]{:S(2)}) async-start(s8[7340032]{0:T(1024)(128)(4,1)} %bitcast.86), calls=%async_computation.7 | async-start | bytes 6291456
  91.2 15.6 %slice-start.2 = ((s8[7340032]{0:T(1024)(128)(4,1)}), s8[4194304]{0:T(1024)(128)(4,1)S(1)}, s32[]{:S(2)}) async-start(s8[7340032]{0:T(1024)(128)(4,1)} %bitcast.88), calls=%async_computation.8 | async-start | bytes 8388608
  100.3 6.5 %slice-start.3 = ((s8[7340032]{0:T(1024)(128)(4,1)}), s8[3145728]{0:T(1024)(128)(4,1)S(1)}, s32[]{:S(2)}) async-start(s8[7340032]{0:T(1024)(128)(4,1)} %bitcast.88), calls=%async_computation.9 | async-start | bytes 6291456
  114.2 0.7 copy-start.9
  138.8 10.5 %copy-start.8 = (f32[128,2]{0,1:T(2,128)S(1)}, f32[128,2]{0,1:T(2,128)}, u32[]{:S(2)}) copy-start(f32[128,2]{0,1:T(2,128)} %param.20) | copy-start | bytes 3076
  142.2 44.5 %all-to-all-start.1 = ((bf16[16,24,2048]{2,1,0:T(8,128)(2,1)}), bf16[16,24,2048]{2,1,0:T(8,128)(2,1)}, u32[]{:S(2)}, u32[]{:S(2)}) async-start(bf16[16,24,2048]{2,1,0:T(8,128)(2,1)} %dynamic-slice_bitcast_fusion), calls=%async_computation.2 | async-start | bytes 3145728 | tf_op jit(solution)/shard_map/all_to_all | solution.py:125
  191.7 8.3 %copy-start.1 = (f32[128,2048]{1,0:T(8,128)S(1)}, f32[128,2048]{1,0:T(8,128)}, u32[]{:S(2)}) copy-start(f32[128,2048]{1,0:T(8,128)} %reduce-scatter.3.cloned.1.call-done) | copy-start | bytes 3145732
  195.1 4.9 %copy-start.3 = (bf16[128,2048]{1,0:T(8,128)(2,1)S(1)}, bf16[128,2048]{1,0:T(8,128)(2,1)}, u32[]{:S(2)}) copy-start(bf16[128,2048]{1,0:T(8,128)(2,1)} %param.17) | copy-start | bytes 1572868
Sparse Core Ops, SparseCore 0:
  20.0 10.3 reduce-scatter.2
  77.4 11.4 all-gather.2
  114.3 24.4 all-reduce.2
